TPU v7x, 512 devices: a whole 4x4x16 slice. The times are simulated.
512 devices in a mesh: ep: 32 (over z, core), tp: 16 (over y, x).
Axes of the slice: x: 4, y: 4, z: 16, core: 2. Of those that a mesh axis runs over, the one named last changes fastest.
Arguments:
- query_rows: bfloat16 [24576, 1024], P('ep', 'tp'), may hold values from -600 to 600
- key_rows: bfloat16 [24576, 1024], P('ep', 'tp'), may hold values from -6 to 6
- value_rows: bfloat16 [24576, 1024], P('ep', 'tp'), may hold values from -6 to 6
- cum_gate: float32 [16, 24576], P('tp'), may hold values from -2458 to 0, as said below
- out_weight: bfloat16 [1024, 2048], P(None, 'tp'), may hold values from -0.1875 to 0.1875
- moe_input: bfloat16 [6144, 2048], P('ep'), may hold values from -6 to 6
- moe_gain: float32 [2048], replicated, may hold values from 0.1 to 1.9
- routes: int32 [6144, 3], P('ep'), may hold values from 0 to 127, all different within a row; in each aligned block of 192 rows (0 to 191, 192 to 383, ...) at most 9 rows name the same one
- route_weight: float32 [6144, 3], P('ep'), may hold values from 0.2 to 1.5
- expert_gate: bfloat16 [128, 2048, 512], P('ep', None, 'tp'), may hold values from -0.125 to 0.125
- expert_up: bfloat16 [128, 2048, 512], P('ep', None, 'tp'), may hold values from -0.125 to 0.125
- expert_down: bfloat16 [128, 512, 2048], P('ep', None, 'tp'), may hold values from -0.25 to 0.25
- shared_gate: bfloat16 [2048, 512], P(None, 'tp'), may hold values from -0.125 to 0.125
- shared_up: bfloat16 [2048, 512], P(None, 'tp'), may hold values from -0.125 to 0.125
- shared_down: bfloat16 [512, 2048], P(None, 'tp'), may hold values from -0.25 to 0.25
Outputs:
- mixer_out: bfloat16 [24576, 2048], P('ep', 'tp')
- moe_out: bfloat16 [6144, 2048], P('ep', 'tp')
Inputs may be any that keep to these rules, and one draw needn't show every extreme that they name: Non-increasing along positions: cum_gate[h, t] is the sum of the log forget gates of head h over positions 0 to t. `routes`: the 3 experts of a token differ. In each aligned block of 192 tokens no expert is named by more than 9 tokens, a bound that some block reaches.
All inputs are finite; a program needn't handle non-finite values.
Results may differ from a plain program's by a relative error of at most 0.0068.
Values may be sent and summed in bfloat16 or wider, within the bound.
No kernel may reach another device: no remote copies, remote signals or barrier semaphores. Data moves between devices by JAX's collectives and lax.ppermute only.
A program may use at most 64 MiB of HBM per device.

v0:
```python
import jax
import jax.numpy as jnp
from jax import lax
from jax.sharding import PartitionSpec as P

HEAD = 64
neg_fill = -1e30
norm_eps = 1e-06


def joined_along(pieces, dim):
    dims = list(pieces.shape[1:])
    dims[dim] *= pieces.shape[0]
    return jnp.moveaxis(pieces, 0, dim).reshape(dims)


def sent_to_all(array, axis):
    copies = jnp.broadcast_to(array, (lax.axis_size(axis), *array.shape))
    return lax.all_to_all(copies, axis, split_axis=0, concat_axis=0, tiled=True)


def collect(array, axis, dim):
    return joined_along(sent_to_all(array, axis), dim)


def local(
    query_rows,
    key_rows,
    value_rows,
    cum_gate,
    out_weight,
    moe_input,
    moe_gain,
    routes,
    route_weight,
    expert_gate,
    expert_up,
    expert_down,
    shared_gate,
    shared_up,
    shared_down,
):
    row_count = query_rows.shape[0]
    width = query_rows.shape[1]
    local_heads = width // HEAD
    scale = HEAD ** (-0.5)
    first_row = lax.axis_index("ep") * row_count
    last_row = first_row + row_count - 1
    query_heads = query_rows.reshape(row_count, local_heads, HEAD)
    query_gate = lax.dynamic_slice_in_dim(cum_gate, first_row, row_count, 1)
    query_pos = first_row + jnp.arange(row_count, dtype=jnp.int32)
    key_value = jnp.concatenate([key_rows, value_rows], axis=1)
    initial = (
        jnp.full((local_heads, row_count), neg_fill, jnp.float32),
        jnp.zeros((local_heads, row_count), jnp.float32),
        jnp.zeros((local_heads, row_count, HEAD), jnp.float32),
    )
    shard_rows = lax.all_gather(key_value, "ep", axis=0, tiled=True)
    piece_len = shard_rows.shape[0]
    key_span = 512

    def one_span(state_in, span_index):
        span_start = span_index * key_span

        def update(state_old):
            running_max, denominator, weighted = state_old
            block = lax.dynamic_slice_in_dim(shard_rows, span_index * key_span, key_span, 0)
            keys_block = block[:, :width].reshape(key_span, local_heads, HEAD)
            values_block = block[:, width:].reshape(key_span, local_heads, HEAD)
            key_gate = lax.dynamic_slice_in_dim(cum_gate, span_start, key_span, 1)
            scores = (
                jnp.einsum(
                    "qhd,khd->hqk", query_heads, keys_block, preferred_element_type=jnp.float32
                )
                * scale
            )
            scores = scores + query_gate[:, :, None] - key_gate[:, None, :]
            causal = (span_start + jnp.arange(key_span, dtype=jnp.int32))[None, :] <= query_pos[
                :, None
            ]
            scores = jnp.where(causal[None], scores, neg_fill)
            new_max = jnp.maximum(running_max, jnp.max(scores, axis=2))
            expon = jnp.where(causal[None], jnp.exp(scores - new_max[:, :, None]), 0.0)
            rescale = jnp.exp(running_max - new_max)
            denominator = denominator * rescale + jnp.sum(expon, axis=2)
            weighted = weighted * rescale[:, :, None] + jnp.einsum(
                "hqk,khd->hqd",
                expon.astype(jnp.bfloat16),
                values_block,
                preferred_element_type=jnp.float32,
            )
            return (new_max, denominator, weighted)

        state_next = lax.cond(span_start <= last_row, update, lambda unchanged: unchanged, state_in)
        return (state_next, None)

    state_out, _ = lax.scan(one_span, initial, jnp.arange(piece_len // key_span, dtype=jnp.int32))
    running_max, denominator, weighted = state_out
    heads_out = (weighted / denominator[:, :, None]).transpose(1, 0, 2).reshape(row_count, width)
    heads_out = heads_out.astype(jnp.bfloat16)
    token_count = moe_input.shape[0]
    top_count = routes.shape[1]
    local_experts = expert_gate.shape[0]
    ep_count = lax.axis_size("ep")
    expert_count = local_experts * ep_count
    capacity = 2 * token_count * top_count // expert_count
    column_count = expert_down.shape[2]
    first_column = lax.axis_index("tp") * column_count
    moe_rows = moe_input.astype(jnp.float32)
    normed = (
        moe_rows
        * lax.rsqrt(jnp.mean(moe_rows * moe_rows, axis=1, keepdims=True) + norm_eps)
        * moe_gain
    ).astype(jnp.bfloat16)
    flat_routes = routes.reshape(-1)
    one_hot = (flat_routes[:, None] == jnp.arange(expert_count, dtype=jnp.int32)[None, :]).astype(
        jnp.int32
    )
    ranks = jnp.sum(jnp.cumsum(one_hot, axis=0) * one_hot, axis=1) - 1
    slot_index = flat_routes * capacity + ranks
    pair_token = jnp.arange(token_count * top_count, dtype=jnp.int32) // top_count
    slot_token = (
        jnp.full((expert_count * capacity,), token_count, jnp.int32).at[slot_index].set(pair_token)
    )
    padded = jnp.concatenate([normed, jnp.zeros((1, normed.shape[1]), jnp.bfloat16)], axis=0)
    outgoing = lax.dynamic_slice_in_dim(padded, first_column, column_count, 1)[slot_token]
    outgoing = outgoing.reshape(ep_count, local_experts, capacity, outgoing.shape[1])
    arrived = lax.all_to_all(outgoing, "ep", split_axis=0, concat_axis=0, tiled=True)
    arrived = lax.all_gather(arrived, "tp", axis=3, tiled=True)
    gate_val = jnp.einsum(
        "aecd,edf->aecf", arrived, expert_gate, preferred_element_type=jnp.float32
    )
    up_val = jnp.einsum("aecd,edf->aecf", arrived, expert_up, preferred_element_type=jnp.float32)
    hidden = (jax.nn.silu(gate_val) * up_val).astype(jnp.bfloat16)
    hidden = collect(hidden, "tp", 3)
    result = jnp.einsum(
        "aecf,efd->aecd", hidden, expert_down, preferred_element_type=jnp.float32
    ).astype(jnp.bfloat16)
    returned = lax.all_to_all(result, "ep", split_axis=0, concat_axis=0, tiled=True)
    picked = returned.reshape(expert_count * capacity, column_count)[slot_index]
    picked = picked.astype(jnp.float32).reshape(token_count, top_count, column_count)
    routed = jnp.sum(picked * route_weight[:, :, None], axis=1)
    shared_hidden = (
        jax.nn.silu(jnp.dot(normed, shared_gate, preferred_element_type=jnp.float32))
        * jnp.dot(normed, shared_up, preferred_element_type=jnp.float32)
    ).astype(jnp.bfloat16)
    mixer_sum = jnp.dot(
        lax.all_gather(heads_out, "tp", axis=1, tiled=True),
        out_weight,
        preferred_element_type=jnp.float32,
    )
    shared_all = lax.all_gather(shared_hidden, "tp", axis=1, tiled=True)
    moe_total = routed + jnp.dot(shared_all, shared_down, preferred_element_type=jnp.float32)
    return (mixer_sum.astype(jnp.bfloat16), moe_total.astype(jnp.bfloat16))


def solution(mesh):
    placed = (
        P("ep", "tp"),
        P("ep", "tp"),
        P("ep", "tp"),
        P("tp", None),
        P(None, "tp"),
        P("ep", None),
        P(),
        P("ep", None),
        P("ep", None),
        P("ep", None, "tp"),
        P("ep", None, "tp"),
        P("ep", None, "tp"),
        P(None, "tp"),
        P(None, "tp"),
        P(None, "tp"),
    )
    return jax.shard_map(
        local, mesh=mesh, in_specs=placed, out_specs=(P("ep", "tp"), P("ep", "tp")), check_vma=False
    )
```

profile of v0, /device:TPU:1, one launch (start us, length us, event | category | flops | bytes accessed | tf_op | source)
XLA Modules:
  0.0 554.8 jit_solution(1330439696241112962)
XLA Ops:
  7.2 0.7 broadcast_multiply_fusion
  8.0 0.8 copy.43
  8.8 1.4 fusion.15
  11.6 4.1 scatter_custom_fusion
  16.0 2.9 gather_fusion
  19.3 40.2 %all_to_all.15 = bf16[32,4,9,128]{3,1,2,0:T(4,128)(2,1)S(1)} all-to-all(bf16[32,4,9,128]{3,1,2,0:T(4,128)(2,1)S(1)} %copy.46), channel_id=1, replica_groups=mesh['ep'=32,'tp'=16] {'ep'}, dimensions={0} | all-to-all | bytes 589824 | tf_op jit(solution)/shard_map/all_to_all | solution.py:128
  59.5 0.8 copy.47
  60.7 0.8 pad_maximum_fusion
  61.6 63.6 %all-gather.7.cloned.1.call-done = bf16[32,4,9,2048]{3,0,2,1:T(8,128)(2,1)} async-done(((bf16[32,4,9,128]{3,0,2,1:T(8,128)(2,1)}), bf16[32,4,9,2048]{3,0,2,1:T(8,128)(2,1)}) %all-gather.7.cloned.1.call-update) | async-done | bytes 4718608 | tf_op jit(solution)/shard_map/all_gather | solution.py:129
  125.2 3.8 convolution_bitcast_fusion.2
  129.1 1.4 fusion.21
  130.5 3.2 broadcast_bitcast_fusion
  133.7 7.8 %reshape.164 = bf16[16,2,18432]{2,1,0:T(2,128)(2,1)} reshape(bf16[16,4,9,32,32]{4,3,2,1,0:T(8,128)(2,1)} %broadcast_bitcast_fusion) | data formatting | bytes 2359296
  141.5 4.8 all-to-all-start.1
  146.6 0.7 constant_dynamic-slice_fusion.1
  147.2 58.1 %all-gather.5.cloned.1.call-done = bf16[24576,128]{1,0:T(8,128)(2,1)} async-done(((bf16[768,128]{1,0:T(8,128)(2,1)}), bf16[24576,128]{1,0:T(8,128)(2,1)}) %all-gather.5.cloned.1.call-update) | async-done | bytes 6291472 | tf_op jit(solution)/shard_map/all_gather | solution.py:58
  205.4 76.2 %while.15 = (s32[]{:T(128)}, f32[1,768]{1,0:T(1,128)S(1)}, f32[1,768]{1,0:T(1,128)S(1)}, f32[1,768,64]{1,2,0:T(8,128)S(1)}, s32[48]{0:T(128)S(1)}, /*index=5*/s3...) while((s32[]{:T(128)}, f32[1,768]{1,0:T(1,128)S(1)}, ...), condition=%wide.region_5.6_spmd.clone, body=%wide.region_0.5_spmd.clone.sunk | while | flops 106270224 | bytes 5566899 | solution.py:97
  205.4 0.6 dynamic_slice.23
  206.7 4.7 conditional.3
  207.4 0.8 constant_dynamic-slice_fusion
  208.1 1.4 fusion.40
  209.6 1.4 fusion.4
  212.6 4.7 conditional.3
  213.3 0.8 constant_dynamic-slice_fusion
  214.1 1.4 fusion.40
  215.5 1.4 fusion.4
  217.3 0.6 dynamic_slice.23
  218.6 4.7 conditional.3
  219.3 0.8 constant_dynamic-slice_fusion
  220.0 1.4 fusion.40
  221.5 1.4 fusion.4
  223.3 0.6 dynamic_slice.23
  224.6 0.6 dynamic_slice.23
  227.2 0.6 dynamic_slice.23
  228.5 0.6 dynamic_slice.23
  229.7 0.6 dynamic_slice.23
  281.6 0.7 divide_convert_fusion
  282.3 3.8 reshape.165
  286.1 3.1 bitcast_bitcast_fusion
  289.2 7.6 %copy.48 = bf16[32,4,9,16,32]{4,3,0,2,1:T(8,128)(2,1)} copy(bf16[32,4,9,16,32]{4,0,2,1,3:T(8,128)(2,1)S(1)} %bitcast_bitcast_fusion) | data formatting | bytes 2359296 | tf_op jit(solution)/shard_map/transpose | solution.py:14
  296.8 6.5 %reshape.124 = bf16[32,4,9,512]{3,0,2,1:T(8,128)(2,1)S(1)} reshape(bf16[32,4,9,16,32]{4,3,0,2,1:T(8,128)(2,1)} %copy.48) | data formatting | bytes 2359296 | tf_op jit(solution)/shard_map/reshape | solution.py:14
  303.8 0.9 copy.49
  304.7 213.7 %all-to-all-start.2 = ((bf16[32,4,9,128]{3,1,2,0:T(4,128)(2,1)}), bf16[32,4,9,128]{3,1,2,0:T(4,128)(2,1)S(1)}, u32[]{:S(2)}, u32[]{:S(2)}) async-start(bf16[32,4,9,128]{3,1,2,0:T(4,128)(2,1)} %copy.49), calls=%async_computation.2 | async-start | bytes 589824 | tf_op jit(solution)/shard_map/all_to_all | solution.py:139
  519.2 20.5 %all_gather.15 = bf16[192,512]{0,1:T(8,128)(2,1)S(1)} all-gather(bf16[192,32]{0,1:T(8,128)(2,1)S(1)} %fusion.27), channel_id=1, replica_groups=mesh['ep'=32,'tp'=16] {'tp'}, dimensions={1}, use_global_device_ids=true | all-gather | bytes 208896 | tf_op jit(solution)/shard_map/all_gather | solution.py:152
  539.7 2.2 all-to-all-done.2
  542.2 1.9 gather_fusion.1
  544.6 0.9 fusion.26
  545.5 2.7 fusion.22
  (228 shorter events, 30.8 us)
Async XLA Ops:
  7.2 296.1 %copy-start = (bf16[4,512,128]{2,1,0:T(8,128)(2,1)S(1)}, bf16[4,512,128]{2,1,0:T(8,128)(2,1)}, u32[]{:S(2)}) copy-start(bf16[4,512,128]{2,1,0:T(8,128)(2,1)} %param.30) | copy-start | bytes 1572868
  7.2 118.0 %all-gather.7.cloned.1.call-start = ((), (), s32[]{:S(2)}) async-start(), calls=%async_computation.4 | async-start | bytes 5013504 | tf_op jit(solution)/shard_map/all_gather | solution.py:129
  10.9 4.8 copy-start.1
  10.9 4.8 copy-start.8
  19.0 41.4 %copy-start.6 = (bf16[768,64]{0,1:T(8,128)(2,1)S(1)}, bf16[768,64]{0,1:T(8,128)(2,1)}, u32[]{:S(2)}) copy-start(bf16[768,64]{0,1:T(8,128)(2,1)} %param.20) | copy-start | bytes 294916
  19.0 41.6 %copy-start.7 = (bf16[768,64]{0,1:T(8,128)(2,1)S(1)}, bf16[768,64]{0,1:T(8,128)(2,1)}, u32[]{:S(2)}) copy-start(bf16[768,64]{0,1:T(8,128)(2,1)} %param.21) | copy-start | bytes 294916
  19.3 105.9 %copy-start.11 = (bf16[4,2048,32]{1,2,0:T(8,128)(2,1)S(1)}, bf16[4,2048,32]{1,2,0:T(8,128)(2,1)}, u32[]{:S(2)}) copy-start(bf16[4,2048,32]{1,2,0:T(8,128)(2,1)} %param.28) | copy-start | bytes 1572868
  60.3 145.0 %all-gather.5.cloned.1.call-start = ((), (), s32[]{:S(2)}) async-start(), calls=%async_computation.3 | async-start | bytes 6488064 | tf_op jit(solution)/shard_map/all_gather | solution.py:58
  61.6 67.5 %copy-start.12 = (bf16[4,2048,32]{1,2,0:T(8,128)(2,1)S(1)}, bf16[4,2048,32]{1,2,0:T(8,128)(2,1)}, u32[]{:S(2)}) copy-start(bf16[4,2048,32]{1,2,0:T(8,128)(2,1)} %param.29) | copy-start | bytes 1572868
  125.2 3.9 copy-start.10
  141.5 63.9 %copy-start.13 = (bf16[768,64]{0,1:T(8,128)(2,1)S(1)}, bf16[768,64]{0,1:T(8,128)(2,1)}, u32[]{:S(2)}) copy-start(bf16[768,64]{0,1:T(8,128)(2,1)} %param.19) | copy-start | bytes 294916
  141.5 140.8 %all-to-all-start.1 = ((bf16[16,2,18432]{2,1,0:T(2,128)(2,1)}), bf16[16,2,18432]{2,1,0:T(2,128)(2,1)S(1)}, u32[]{:S(2)}, u32[]{:S(2)}) async-start(bf16[16,2,18432]{2,1,0:T(2,128)(2,1)} %reshape.164), calls=%async_computation.1 | async-start | bytes 2359296 | tf_op jit(solution)/shard_map/all_to_all | solution.py:19
  146.3 399.2 %all-gather.9.cloned.1.call-start = ((), (), s32[]{:S(2)}) async-start(), calls=%async_computation.5 | async-start | bytes 1671168 | tf_op jit(solution)/shard_map/all_gather | solution.py:148
  303.3 215.1 %copy-start.9 = (f32[192,3]{0,1:T(4,128)S(1)}, f32[192,3]{0,1:T(4,128)}, u32[]{:S(2)}) copy-start(f32[192,3]{0,1:T(4,128)} %param.27) | copy-start | bytes 6916
  303.3 215.2 %copy-start.4 = (bf16[2048,32]{0,1:T(8,128)(2,1)S(1)}, bf16[2048,32]{0,1:T(8,128)(2,1)}, u32[]{:S(2)}) copy-start(bf16[2048,32]{0,1:T(8,128)(2,1)} %param.31) | copy-start | bytes 393220
  303.8 215.1 %copy-start.5 = (bf16[2048,32]{0,1:T(8,128)(2,1)S(1)}, bf16[2048,32]{0,1:T(8,128)(2,1)}, u32[]{:S(2)}) copy-start(bf16[2048,32]{0,1:T(8,128)(2,1)} %param.32) | copy-start | bytes 393220
  304.7 237.3 %all-to-all-start.2 = ((bf16[32,4,9,128]{3,1,2,0:T(4,128)(2,1)}), bf16[32,4,9,128]{3,1,2,0:T(4,128)(2,1)S(1)}, u32[]{:S(2)}, u32[]{:S(2)}) async-start(bf16[32,4,9,128]{3,1,2,0:T(4,128)(2,1)} %copy.49), calls=%async_computation.2 | async-start | bytes 589824 | tf_op jit(solution)/shard_map/all_to_all | solution.py:139
  542.1 2.6 copy-start.3
  542.2 3.3 copy-start.2
Sparse Core Ops, SparseCore 0:
  60.4 64.7 all-gather.6
  127.9 77.4 all-gather.4
  282.4 260.1 all-gather.8
where the time goes:
time: 559 us; the launch traced here: 555 us
  starting transfers between devices  219 us (39%)
  waiting for transfers between devices  124 us (22%)
  local copies, waits for them, and re-layouts  76.5 us (14%)
  blocking collectives  60.7 us (11%)
  loops' own time  36.1 us (6%)
  matrix products  18.3 us (3%)
  between operations  14.2 us (3%)
  other arithmetic  6.13 us (1%)
    all_to_all x1, starting transfers between devices, local(): lax.all_to_all(result, 'ep', split_axis=0, concat_axis=0, tiled=True)  214 us
    all_gather x1, waiting for transfers between devices, local(): arrived = lax.all_gather(arrived, 'tp', axis=3, tiled=True)  63.6 us
    all_gather x1, waiting for transfers between devices, local(): shard_rows = lax.all_gather(key_value, 'ep', axis=0, tiled=True)  58.1 us
    all_to_all x1, blocking collectives, local(): lax.all_to_all(outgoing, 'ep', split_axis=0, concat_axis=0, tiled=True)  40.2 us
    another operation x1, loops' own time, local(): lax.scan(one_span, initial, jnp.arange(piece_len // key_span, dtype=jnp.i...  33.2 us
    dynamic_slice x48, local copies, waits for them, and re-layouts, local(): lax.scan(one_span, initial, jnp.arange(piece_len // key_span, dtype=jnp.i...  28.1 us
    all_gather x1, blocking collectives, local(): shared_all = lax.all_gather(shared_hidden, 'tp', axis=1, tiled=True)  20.5 us
    unnamed x35, local copies, waits for them, and re-layouts  16.1 us
  transfers between devices with their start and end apart: 5, of which 3 were waited for; matrix products, arithmetic and copies ran while one was open for 15% of the time, Pallas kernels for 0%

commit v1 on v0

--- a/solution.py
+++ b/solution.py
@@ -126,7 +126,9 @@
     outgoing = lax.dynamic_slice_in_dim(padded, first_column, column_count, 1)[slot_token]
     outgoing = outgoing.reshape(ep_count, local_experts, capacity, outgoing.shape[1])
     arrived = lax.all_to_all(outgoing, "ep", split_axis=0, concat_axis=0, tiled=True)
-    arrived = lax.all_gather(arrived, "tp", axis=3, tiled=True)
+    arrived = jnp.concatenate(
+        lax.all_to_all(jnp.stack([arrived] * lax.axis_size("tp")), "tp", 0, 0), axis=3
+    )
     gate_val = jnp.einsum(
         "aecd,edf->aecf", arrived, expert_gate, preferred_element_type=jnp.float32
     )

time: 559 us -> 494 us (0.88)
  waiting for transfers between devices: 124 us -> 2.22 us
  blocking collectives: 60.7 us -> 126 us
  starting transfers between devices: 219 us -> 212 us
    all_gather x1 -> x0, waiting for transfers between devices: 63.6 us -> none  [local(): arrived = lax.all_gather(arrived, 'tp', axis=3, tiled=True)]
    all_to_all x0 -> x1, blocking collectives: none -> 63.3 us  [local(): lax.all_to_all(jnp.stack([arrived] * lax.axis_size('tp')), 'tp', 0, 0)]
    all_gather x1, waiting for transfers between devices: 58.1 us -> 0.01 us  [local(): shard_rows = lax.all_gather(key_value, 'ep', axis=0, tiled=True)]
    all_to_all x1, starting transfers between devices: 214 us -> 208 us  [local(): lax.all_to_all(result, 'ep', split_axis=0, concat_axis=0, tiled=True)]
    unnamed x35 -> x29, local copies, waits for them, and re-layouts: 16.1 us -> 18 us
  transfers between devices with their start and end apart: 5 -> 4, of which waited for: 3 -> 1; matrix products, arithmetic and copies ran while one was open for 15% -> 19% of each run, Pallas kernels for 0% -> 0%
where the time goes in v1:
time: 494 us; the launch traced here: 490 us
  starting transfers between devices  212 us (43%)
  blocking collectives  126 us (26%)
  local copies, waits for them, and re-layouts  78.5 us (16%)
  loops' own time  36.1 us (7%)
  matrix products  15.8 us (3%)
  between operations  14.5 us (3%)
  other arithmetic  4.95 us (1%)
    all_to_all x1, starting transfers between devices, local(): lax.all_to_all(result, 'ep', split_axis=0, concat_axis=0, tiled=True)  208 us
    all_to_all x1, blocking collectives, local(): lax.all_to_all(jnp.stack([arrived] * lax.axis_size('tp')), 'tp', 0, 0)  63.3 us
    all_to_all x1, blocking collectives, local(): lax.all_to_all(outgoing, 'ep', split_axis=0, concat_axis=0, tiled=True)  41.7 us
    another operation x1, loops' own time, local(): lax.scan(one_span, initial, jnp.arange(piece_len // key_span, dtype=jnp.i...  33.2 us
    dynamic_slice x48, local copies, waits for them, and re-layouts, local(): lax.scan(one_span, initial, jnp.arange(piece_len // key_span, dtype=jnp.i...  28.1 us
    all_gather x1, blocking collectives, local(): shared_all = lax.all_gather(shared_hidden, 'tp', axis=1, tiled=True)  20.5 us
    unnamed x29, local copies, waits for them, and re-layouts  18 us
    transpose x2, local copies, waits for them, and re-layouts, joined_along(): return jnp.moveaxis(pieces, 0, dim).reshape(dims)  10.7 us
  transfers between devices with their start and end apart: 4, of which 1 were waited for; matrix products, arithmetic and copies ran while one was open for 19% of the time, Pallas kernels for 0%

profile of v1, /device:TPU:1, one launch (start us, length us, event | category | flops | bytes accessed | tf_op | source)
XLA Modules:
  0.0 489.6 jit_solution(5181445701204837118)
XLA Ops:
  7.2 1.1 copy.43
  8.3 1.1 copy.44
  9.4 0.8 pad_maximum_fusion
  10.2 0.8 copy.46
  11.0 0.7 broadcast_multiply_fusion
  13.2 4.1 scatter_custom_fusion
  17.9 2.9 gather_fusion
  21.1 41.7 %all_to_all.20 = bf16[32,4,9,128]{3,1,2,0:T(4,128)(2,1)S(1)} all-to-all(bf16[32,4,9,128]{3,1,2,0:T(4,128)(2,1)S(1)} %copy.49), channel_id=1, replica_groups=mesh['ep'=32,'tp'=16] {'ep'}, dimensions={0} | all-to-all | bytes 589824 | tf_op jit(solution)/shard_map/all_to_all | solution.py:128
  62.9 1.0 stack.2
  63.8 63.3 %all_to_all.21 = bf16[16,32,4,9,128]{4,1,3,2,0:T(8,128)(2,1)S(1)} all-to-all(bf16[16,32,4,9,128]{4,1,3,2,0:T(8,128)(2,1)S(1)} %stack.2), channel_id=1, replica_groups=mesh['ep'=32,'tp'=16] {'tp'}, dimensions={0} | all-to-all | bytes 9437184 | tf_op jit(solution)/shard_map/all_to_all | solution.py:130
  127.2 1.3 fusion.26
  128.5 1.4 fusion.35
  129.9 3.2 broadcast_bitcast_fusion
  133.1 7.8 %reshape.174 = bf16[16,2,18432]{2,1,0:T(2,128)(2,1)} reshape(bf16[16,4,9,32,32]{4,3,2,1,0:T(8,128)(2,1)} %broadcast_bitcast_fusion) | data formatting | bytes 2359296
  140.9 3.8 all-to-all-start.2
  145.0 0.7 constant_dynamic-slice_fusion.1
  145.7 76.2 %while.15 = (s32[]{:T(128)}, f32[1,768]{1,0:T(1,128)S(1)}, f32[1,768]{1,0:T(1,128)S(1)}, f32[1,768,64]{1,2,0:T(8,128)S(1)}, s32[48]{0:T(128)S(1)}, /*index=5*/s3...) while((s32[]{:T(128)}, f32[1,768]{1,0:T(1,128)S(1)}, ...), condition=%wide.region_5.6_spmd.clone, body=%wide.region_0.5_spmd.clone.sunk | while | flops 106270224 | bytes 5566899 | solution.py:97
  145.8 0.6 dynamic_slice.23
  147.0 4.7 conditional.3
  147.7 0.8 constant_dynamic-slice_fusion
  148.5 1.4 fusion.56
  149.9 1.4 fusion.4
  151.7 0.6 dynamic_slice.23
  153.0 4.7 conditional.3
  153.7 0.8 constant_dynamic-slice_fusion
  154.5 1.4 fusion.56
  155.9 1.4 fusion.4
  157.7 0.6 dynamic_slice.23
  158.9 4.7 conditional.3
  159.6 0.8 constant_dynamic-slice_fusion
  160.4 1.4 fusion.56
  161.8 1.4 fusion.4
  163.6 0.6 dynamic_slice.23
  164.9 0.6 dynamic_slice.23
  166.2 0.6 dynamic_slice.23
  167.5 0.6 dynamic_slice.23
  222.0 0.7 divide_convert_fusion
  222.7 3.8 reshape.175
  226.4 3.1 bitcast_bitcast_fusion
  229.6 7.6 %copy.52 = bf16[32,4,9,16,32]{4,3,0,2,1:T(8,128)(2,1)} copy(bf16[32,4,9,16,32]{4,0,2,1,3:T(8,128)(2,1)S(1)} %bitcast_bitcast_fusion) | data formatting | bytes 2359296 | tf_op jit(solution)/shard_map/transpose | solution.py:14
  237.2 6.5 %reshape.134 = bf16[32,4,9,512]{3,0,2,1:T(8,128)(2,1)S(1)} reshape(bf16[32,4,9,16,32]{4,3,0,2,1:T(8,128)(2,1)} %copy.52) | data formatting | bytes 2359296 | tf_op jit(solution)/shard_map/reshape | solution.py:14
  244.2 0.9 copy.53
  245.0 207.8 %all-to-all-start.3 = ((bf16[32,4,9,128]{3,1,2,0:T(4,128)(2,1)}), bf16[32,4,9,128]{3,1,2,0:T(4,128)(2,1)S(1)}, u32[]{:S(2)}, u32[]{:S(2)}) async-start(bf16[32,4,9,128]{3,1,2,0:T(4,128)(2,1)} %copy.53), calls=%async_computation.3 | async-start | bytes 589824 | tf_op jit(solution)/shard_map/all_to_all | solution.py:141
  453.7 20.5 %all_gather.11 = bf16[192,512]{0,1:T(8,128)(2,1)S(1)} all-gather(bf16[192,32]{0,1:T(8,128)(2,1)S(1)} %fusion.43), channel_id=1, replica_groups=mesh['ep'=32,'tp'=16] {'tp'}, dimensions={1}, use_global_device_ids=true | all-gather | bytes 208896 | tf_op jit(solution)/shard_map/all_gather | solution.py:154
  474.3 2.2 all-to-all-done.3
  476.7 1.9 gather_fusion.1
  479.1 0.9 fusion.42
  480.0 2.7 fusion.38
  (221 shorter events, 30.7 us)
Async XLA Ops:
  7.2 236.5 %copy-start = (bf16[4,512,128]{2,1,0:T(8,128)(2,1)S(1)}, bf16[4,512,128]{2,1,0:T(8,128)(2,1)}, u32[]{:S(2)}) copy-start(bf16[4,512,128]{2,1,0:T(8,128)(2,1)} %param.30) | copy-start | bytes 1572868
  7.2 138.5 %all-gather.4.cloned.1.call-start = ((), (), s32[]{:S(2)}) async-start(), calls=%async_computation.4 | async-start | bytes 6488064 | tf_op jit(solution)/shard_map/all_gather | solution.py:58
  12.5 4.8 copy-start.1
  12.7 4.9 copy-start.6
  63.8 63.3 %copy-start.8 = (bf16[4,2048,32]{1,2,0:T(8,128)(2,1)S(1)}, bf16[4,2048,32]{1,2,0:T(8,128)(2,1)}, u32[]{:S(2)}) copy-start(bf16[4,2048,32]{1,2,0:T(8,128)(2,1)} %param.28) | copy-start | bytes 1572868
  127.2 1.4 copy-start.9
  140.9 4.8 copy-start.10
  140.9 81.7 %all-to-all-start.2 = ((bf16[16,2,18432]{2,1,0:T(2,128)(2,1)}), bf16[16,2,18432]{2,1,0:T(2,128)(2,1)S(1)}, u32[]{:S(2)}, u32[]{:S(2)}) async-start(bf16[16,2,18432]{2,1,0:T(2,128)(2,1)} %reshape.174), calls=%async_computation.2 | async-start | bytes 2359296 | tf_op jit(solution)/shard_map/all_to_all | solution.py:19
  144.8 335.2 %all-gather.6.cloned.1.call-start = ((), (), s32[]{:S(2)}) async-start(), calls=%async_computation.5 | async-start | bytes 1671168 | tf_op jit(solution)/shard_map/all_gather | solution.py:150
  243.6 209.2 %copy-start.7 = (f32[192,3]{0,1:T(4,128)S(1)}, f32[192,3]{0,1:T(4,128)}, u32[]{:S(2)}) copy-start(f32[192,3]{0,1:T(4,128)} %param.27) | copy-start | bytes 6916
  243.7 209.3 %copy-start.4 = (bf16[2048,32]{0,1:T(8,128)(2,1)S(1)}, bf16[2048,32]{0,1:T(8,128)(2,1)}, u32[]{:S(2)}) copy-start(bf16[2048,32]{0,1:T(8,128)(2,1)} %param.31) | copy-start | bytes 393220
  244.2 209.2 %copy-start.5 = (bf16[2048,32]{0,1:T(8,128)(2,1)S(1)}, bf16[2048,32]{0,1:T(8,128)(2,1)}, u32[]{:S(2)}) copy-start(bf16[2048,32]{0,1:T(8,128)(2,1)} %param.32) | copy-start | bytes 393220
  245.0 231.4 %all-to-all-start.3 = ((bf16[32,4,9,128]{3,1,2,0:T(4,128)(2,1)}), bf16[32,4,9,128]{3,1,2,0:T(4,128)(2,1)S(1)}, u32[]{:S(2)}, u32[]{:S(2)}) async-start(bf16[32,4,9,128]{3,1,2,0:T(4,128)(2,1)} %copy.53), calls=%async_computation.3 | async-start | bytes 589824 | tf_op jit(solution)/shard_map/all_to_all | solution.py:141
  476.6 2.6 copy-start.3
  476.7 3.3 copy-start.2
Sparse Core Ops, SparseCore 0:
  10.7 92.6 all-gather.3
  222.8 254.3 all-gather.5
